TPU v7x, 512 devices: a whole 4x8x8 slice. The times are simulated.
512 devices in a mesh: dp: 4 (over x), kv: 64 (over z, y), tp: 2 (over core).
Axes of the slice: x: 4, y: 8, z: 8, core: 2. Of those that a mesh axis runs over, the one named last changes fastest.
Arguments:
- tokens: bfloat16 [256, 4096], P('dp', ('kv', 'tp')), parts along dimension 0, may hold values from -16 to 16
- mix_gain: float32 [4096], replicated, may hold values from 0.1 to 1.9
- w_query: bfloat16 [4096, 2048], P('kv', 'tp'), may hold values from -0.09375 to 0.09375
- w_key: bfloat16 [4096, 2048], P('kv', 'tp'), may hold values from -0.09375 to 0.09375
- w_value: bfloat16 [4096, 4096], P('kv', 'tp'), may hold values from -0.09375 to 0.09375
- w_igate: bfloat16 [4096, 16], replicated, may hold values from -0.09375 to 0.09375
- w_fgate: bfloat16 [4096, 16], replicated, may hold values from -0.09375 to 0.09375
- igate_bias: float32 [16], replicated, may hold values from -3 to 1
- fgate_bias: float32 [16], replicated, may hold values from -2 to 5
- memory: float32 [256, 16, 256, 128], P(('dp', 'kv'), 'tp'), parts along dimension 0, may hold values from -6 to 6
- normalizer: float32 [256, 16, 128], P(('dp', 'kv'), 'tp'), parts along dimension 0, may hold values from -6 to 6
- stabilizer: float32 [256, 16], P(('dp', 'kv'), 'tp'), parts along dimension 0, may hold values from -3 to 3
- w_output: bfloat16 [4096, 4096], P('tp', 'kv'), may hold values from -0.09375 to 0.09375
- mlp_gain: float32 [4096], replicated, may hold values from 0.1 to 1.9
- w_up: bfloat16 [4096, 16384], P(None, ('kv', 'tp')), may hold values from -0.09375 to 0.09375
- w_down: bfloat16 [16384, 4096], P(('kv', 'tp')), may hold values from -0.1875 to 0.1875
Outputs:
- new_tokens: bfloat16 [256, 4096], P('dp', ('kv', 'tp')), parts along dimension 0
- new_memory: float32 [256, 16, 256, 128], P(('dp', 'kv'), 'tp'), parts along dimension 0
- new_normalizer: float32 [256, 16, 128], P(('dp', 'kv'), 'tp'), parts along dimension 0
- new_stabilizer: float32 [256, 16], P(('dp', 'kv'), 'tp'), parts along dimension 0
There are 4 independent parts, one for each index of `dp`. A program takes and returns all parts, laid end to end along the dimension named above; an argument that names none is the same for every part. Nothing has to cross between parts.
All inputs are finite; a program needn't handle non-finite values.
Results may differ from a plain program's by a relative error of at most 0.019.
Values may be sent and summed in bfloat16 or wider, within the bound.
No kernel may reach another device: no remote copies, remote signals or barrier semaphores. Data moves between devices by JAX's collectives and lax.ppermute only.
A program may use at most 64 MiB of HBM per device.

v0:
```python
import jax
import jax.numpy as jnp
from jax import lax
from jax.sharding import PartitionSpec as P

DV = 256
DQK = 128
norm_eps = 1e-06


def cut_along(shard, dim, length):
    before, after = (shard.shape[:dim], shard.shape[dim + 1 :])
    return jnp.moveaxis(shard.reshape(*before, length, -1, *after), dim, 0)


def summed_on_arrival(shard, axis, dim):
    length = lax.axis_size(axis)
    tiles = lax.all_to_all(cut_along(shard, dim, length), axis, 0, 0, tiled=True)
    return jnp.sum(tiles.astype(jnp.float32), axis=0)


def from_everyone(shard, axis):
    length = lax.axis_size(axis)
    return lax.all_to_all(
        jnp.broadcast_to(shard[None], (length, *shard.shape)), axis, 0, 0, tiled=True
    )


def joined_along(tiles, dim):
    dims = list(tiles.shape[1:])
    dims[dim] *= tiles.shape[0]
    return jnp.moveaxis(tiles, 0, dim).reshape(dims)


def collect(shard, axis, dim):
    tiles = from_everyone(shard, axis)
    return joined_along(tiles, dim)


def of_everyone(shard, axis):
    return from_everyone(shard, axis).astype(jnp.float32).sum(axis=0)


def rms_normed(rows, gain):
    wide_rows = rows.astype(jnp.float32)
    scale = lax.rsqrt(jnp.mean(wide_rows * wide_rows, axis=-1, keepdims=True) + norm_eps)
    return (wide_rows * scale * gain).astype(jnp.bfloat16)


def on_device(
    tokens,
    mix_gain,
    w_query,
    w_key,
    w_value,
    w_igate,
    w_fgate,
    igate_bias,
    fgate_bias,
    memory,
    normalizer,
    stabilizer,
    w_output,
    mlp_gain,
    w_up,
    w_down,
):
    kv_count = lax.axis_size("kv")
    tp_count = lax.axis_size("tp")
    kv_index = lax.axis_index("kv")
    tp_index = lax.axis_index("tp")
    own_rows = memory.shape[0]
    head_count = memory.shape[1]
    whole_rows = lax.all_gather(tokens, ("kv", "tp"), axis=1, tiled=True)
    wide_rows = whole_rows.astype(jnp.float32)
    normed = rms_normed(whole_rows, mix_gain)
    row_span = w_query.shape[0]
    own_cols = lax.dynamic_slice_in_dim(normed, kv_index * row_span, row_span, 1)
    joined = summed_on_arrival(
        jnp.concatenate(
            [
                jnp.dot(own_cols, w_query, preferred_element_type=jnp.float32),
                jnp.dot(own_cols, w_key, preferred_element_type=jnp.float32),
                jnp.dot(own_cols, w_value, preferred_element_type=jnp.float32),
            ],
            axis=1,
        ).astype(jnp.bfloat16),
        "kv",
        0,
    )
    query_cols = w_query.shape[1]
    queries = joined[:, :query_cols].reshape(own_rows, head_count, DQK) * DQK ** (-0.5)
    key_rows = joined[:, query_cols : 2 * query_cols].reshape(own_rows, head_count, DQK)
    values = joined[:, 2 * query_cols :].reshape(own_rows, head_count, DV)
    own_normed = lax.dynamic_slice_in_dim(normed, kv_index * own_rows, own_rows, 0)
    igate_cols = lax.dynamic_slice_in_dim(w_igate, tp_index * head_count, head_count, 1)
    fgate_cols = lax.dynamic_slice_in_dim(w_fgate, tp_index * head_count, head_count, 1)
    ibias_own = lax.dynamic_slice_in_dim(igate_bias, tp_index * head_count, head_count, 0)
    fbias_own = lax.dynamic_slice_in_dim(fgate_bias, tp_index * head_count, head_count, 0)
    input_gate = jnp.dot(own_normed, igate_cols, preferred_element_type=jnp.float32) + ibias_own
    log_forget = jax.nn.log_sigmoid(
        jnp.dot(own_normed, fgate_cols, preferred_element_type=jnp.float32) + fbias_own
    )
    carried = log_forget + stabilizer
    new_stabilizer = jnp.maximum(carried, input_gate)
    keep_weight = jnp.exp(carried - new_stabilizer)
    fresh_weight = jnp.exp(input_gate - new_stabilizer)
    recall = jnp.einsum("bhvd,bhd->bhv", memory, queries, precision=lax.Precision.HIGHEST)
    match_score = jnp.sum(queries * key_rows, axis=-1)
    numerator = keep_weight[..., None] * recall + (fresh_weight * match_score)[..., None] * values
    denominator = keep_weight * jnp.sum(normalizer * queries, axis=-1) + fresh_weight * match_score
    floor_value = jnp.maximum(jnp.abs(denominator), jnp.exp(-new_stabilizer))
    cell_out = (
        (numerator / floor_value[..., None]).astype(jnp.bfloat16).reshape(own_rows, head_count * DV)
    )
    new_memory = (
        keep_weight[..., None, None] * memory
        + fresh_weight[..., None, None] * values[..., :, None] * key_rows[..., None, :]
    )
    new_normalizer = keep_weight[..., None] * normalizer + fresh_weight[..., None] * key_rows
    partial_value = jnp.dot(
        collect(cell_out, "kv", 0), w_output, preferred_element_type=jnp.float32
    )
    block_cols = partial_value.shape[1]
    pair_total = of_everyone(partial_value.astype(jnp.bfloat16), "tp").astype(jnp.float32)
    local_rows = lax.dynamic_slice_in_dim(wide_rows, kv_index * block_cols, block_cols, 1)
    middle_block = (local_rows + pair_total).astype(jnp.bfloat16)
    middle = collect(middle_block, "kv", 1)
    mixer_in = rms_normed(middle, mlp_gain)
    up_rows = jnp.dot(mixer_in, w_up, preferred_element_type=jnp.float32)
    activation = jnp.square(jax.nn.relu(up_rows)).astype(jnp.bfloat16)
    thin_cols = tokens.shape[1]
    hidden_rows = w_down.shape[0]
    reordered = jnp.transpose(
        w_down.reshape(hidden_rows, kv_count, tp_count, thin_cols), (0, 2, 1, 3)
    ).reshape(hidden_rows, tp_count * kv_count * thin_cols)
    chip_sums = summed_on_arrival(
        lax.dot_general(
            reordered, activation, (((0,), (1,)), ((), ())), preferred_element_type=jnp.float32
        ).astype(jnp.bfloat16),
        "tp",
        0,
    )
    down_cols = summed_on_arrival(chip_sums.astype(jnp.bfloat16), "kv", 0)
    middle_own = lax.dynamic_slice_in_dim(
        middle, (kv_index * tp_count + tp_index) * thin_cols, thin_cols, 1
    )
    new_tokens = (middle_own.astype(jnp.float32) + down_cols.T).astype(jnp.bfloat16)
    return (new_tokens, new_memory, new_normalizer, new_stabilizer)


def solution(mesh):
    in_specs = (
        P("dp", ("kv", "tp")),
        P(),
        P("kv", "tp"),
        P("kv", "tp"),
        P("kv", "tp"),
        P(),
        P(),
        P(),
        P(),
        P(("dp", "kv"), "tp", None, None),
        P(("dp", "kv"), "tp", None),
        P(("dp", "kv"), "tp"),
        P("tp", "kv"),
        P(),
        P(None, ("kv", "tp")),
        P(("kv", "tp"), None),
    )
    out_specs = (
        P("dp", ("kv", "tp")),
        P(("dp", "kv"), "tp", None, None),
        P(("dp", "kv"), "tp", None),
        P(("dp", "kv"), "tp"),
    )
    return jax.shard_map(
        on_device, mesh=mesh, in_specs=in_specs, out_specs=out_specs, check_vma=False
    )
```

profile of v0, /device:TPU:4, one launch (start us, length us, event | category | flops | bytes accessed | tf_op | source)
XLA Modules:
  0.0 191.2 jit_solution(15945729594412308125)
XLA Ops:
  0.6 58.2 %all_gather.3 = bf16[64,4096]{0,1:T(8,128)(2,1)S(1)} all-gather(bf16[64,32]{0,1:T(8,128)(2,1)} %param.16), channel_id=1, replica_groups=mesh['dp'=4,'kv'=64,'tp'=2] {'kv','tp'}, dimensions={1}, use_global_device_ids=true | all-gather | bytes 528384 | tf_op jit(solution)/shard_map/all_gather | solution.py:74
  58.9 0.3 copy.41
  59.2 0.2 multiply_reduce_fusion.1
  59.6 0.2 multiply_convert_fusion.3
  59.8 0.4 copy-done.3
  60.1 0.3 fusion
  60.4 0.2 fusion.2
  60.7 0.2 fusion.1
  61.0 0.5 broadcast.126
  61.5 1.0 reduce.9
  62.6 1.2 reshape.279
  63.7 7.4 %all-to-all-start = ((bf16[64,2,2048]{2,1,0:T(2,128)(2,1)}), bf16[64,2,2048]{2,1,0:T(2,128)(2,1)S(1)}, u32[]{:S(2)}, u32[]{:S(2)}) async-start(bf16[64,2,2048]{2,1,0:T(2,128)(2,1)} %reshape.279), calls=%async_computation | async-start | bytes 1048576 | tf_op jit(solution)/shard_map/all_to_all | solution.py:18
  71.2 1.0 fusion.8
  72.2 1.0 bitcast_add_fusion.1
  73.3 17.3 %all-to-all-done = bf16[64,2,2048]{2,1,0:T(2,128)(2,1)S(1)} async-done(((bf16[64,2,2048]{2,1,0:T(2,128)(2,1)}), bf16[64,2,2048]{2,1,0:T(2,128)(2,1)S(1)}, u32[]{:S(2)}, u32[]{:S(2)}) %all-to-all-start) | async-done | bytes 524320 | tf_op jit(solution)/shard_map/all_to_all | solution.py:18
  90.6 1.8 reshape.280
  92.3 2.4 %convert_reduce_fusion.1 = f32[4096]{0:T(1024)S(1)} fusion(bf16[64,1,4096]{2,1,0:T(2,128)(2,1)} %reshape.280), kind=kLoop, calls=%fused_computation.25 | loop fusion | flops 520192 | bytes 540672 | tf_op jit(solution)/shard_map/reduce_sum | solution.py:19
  94.8 1.0 fusion.9
  95.7 0.8 multiply_reduce_fusion.3
  96.7 0.3 broadcast_in_dim.9
  97.0 2.2 %reduce.10 = bf16[64,2048]{1,0:T(8,128)(2,1)S(1)} reduce(bf16[64,1,2048]{2,1,0:T(2,128)(2,1)S(1)} %broadcast_in_dim.9, bf16[]{:T(256)} %broadcast.126), dimensions={1}, to_apply=%broadcast_in_dim.9.reduce_sub_computation | reduce | bytes 524290 | tf_op jit(solution)/shard_map/broadcast_in_dim | solution.py:25
  99.1 0.9 reshape.281
  100.0 6.0 %all-to-all-start.1 = ((bf16[64,2,1024]{2,1,0:T(2,128)(2,1)}), bf16[64,2,1024]{2,1,0:T(2,128)(2,1)S(1)}, u32[]{:S(2)}, u32[]{:S(2)}) async-start(bf16[64,2,1024]{2,1,0:T(2,128)(2,1)} %reshape.281), calls=%async_computation.1 | async-start | bytes 524288 | tf_op jit(solution)/shard_map/all_to_all | solution.py:24
  106.0 1.0 convert_element_type.60
  107.1 13.3 %all-to-all-done.1 = bf16[64,2,1024]{2,1,0:T(2,128)(2,1)S(1)} async-done(((bf16[64,2,1024]{2,1,0:T(2,128)(2,1)}), bf16[64,2,1024]{2,1,0:T(2,128)(2,1)S(1)}, u32[]{:S(2)}, u32[]{:S(2)}) %all-to-all-start.1) | async-done | bytes 262176 | tf_op jit(solution)/shard_map/all_to_all | solution.py:24
  120.4 0.2 reshape.282
  120.6 0.3 convolution_convert_fusion.4
  121.0 3.7 %all_to_all.30 = bf16[2,2,2048]{2,1,0:T(2,128)(2,1)S(1)} all-to-all(bf16[2,2,2048]{2,1,0:T(2,128)(2,1)S(1)} %reshape.283), channel_id=1, replica_groups=mesh['dp'=4,'kv'=64,'tp'=2] {'tp'}, dimensions={0} | all-to-all | bytes 32768 | tf_op jit(solution)/shard_map/all_to_all | solution.py:24
  124.9 0.8 add_convert_fusion
  125.8 0.3 broadcast_bitcast_fusion
  126.1 1.6 reshape.285
  127.6 5.5 %all-to-all-start.3 = ((bf16[64,2,2048]{2,1,0:T(2,128)(2,1)}), bf16[64,2,2048]{2,1,0:T(2,128)(2,1)}, u32[]{:S(2)}, u32[]{:S(2)}) async-start(bf16[64,2,2048]{2,1,0:T(2,128)(2,1)} %reshape.285), calls=%async_computation.3 | async-start | bytes 1048576 | tf_op jit(solution)/shard_map/all_to_all | solution.py:24
  133.1 1.6 copy.44
  134.7 1.1 copy.45
  135.8 16.3 %all-to-all-done.3 = bf16[64,2,2048]{2,1,0:T(2,128)(2,1)} async-done(((bf16[64,2,2048]{2,1,0:T(2,128)(2,1)}), bf16[64,2,2048]{2,1,0:T(2,128)(2,1)}, u32[]{:S(2)}, u32[]{:S(2)}) %all-to-all-start.3) | async-done | bytes 524320 | tf_op jit(solution)/shard_map/all_to_all | solution.py:24
  152.1 2.3 %reshape.286 = bf16[64,64,64]{2,1,0:T(8,128)(2,1)S(1)} reshape(bf16[64,2,2048]{2,1,0:T(2,128)(2,1)} %all-to-all-done.3) | data formatting | bytes 1048576
  154.4 0.6 multiply_reduce_fusion
  154.9 3.5 %convolution_convert_fusion = bf16[64,4096]{1,0:T(8,128)(2,1)} fusion(bf16[128,4096]{0,1:T(8,128)(2,1)} %bitcast.116, bf16[4096,128]{1,0:T(8,128)(2,1)S(1)} %copy-done, bf16[64,4096]{0,1:T(8,128)(2,1)S(1)} %bitcast.113, f32[4096]{0:T(1024)S(1)} %copy-done.7, f32[64]{0:T(128)S(1)} %add_rsqrt_fusion), kind=kOutput, calls=%fused_computation | convolution fusion | flops 135553024 | bytes 3162368 | tf_op jit(solution)/shard_map/dot_general | solution.py:138
  158.4 1.1 copy.63
  159.5 4.9 %all_to_all.31 = bf16[2,2048,64]{1,2,0:T(8,128)(2,1)} all-to-all(bf16[2,2048,64]{1,2,0:T(8,128)(2,1)S(1)} %bitcast.118), channel_id=1, replica_groups=mesh['dp'=4,'kv'=64,'tp'=2] {'tp'}, dimensions={0} | all-to-all | bytes 1048576 | tf_op jit(solution)/shard_map/all_to_all | solution.py:18
  164.4 1.1 reduce_sum.90
  165.6 1.0 copy.48
  166.6 2.1 %reshape.287 = bf16[64,2,1024]{2,1,0:T(2,128)(2,1)} reshape(bf16[64,32,64]{2,1,0:T(8,128)(2,1)} %bitcast.117) | data formatting | bytes 524288
  168.6 6.2 %all-to-all-start.5 = ((bf16[64,2,1024]{2,1,0:T(2,128)(2,1)}), bf16[64,2,1024]{2,1,0:T(2,128)(2,1)S(1)}, u32[]{:S(2)}, u32[]{:S(2)}) async-start(bf16[64,2,1024]{2,1,0:T(2,128)(2,1)} %reshape.287), calls=%async_computation.5 | async-start | bytes 524288 | tf_op jit(solution)/shard_map/all_to_all | solution.py:18
  174.9 1.3 multiply_add_fusion
  176.2 13.9 %all-to-all-done.5 = bf16[64,2,1024]{2,1,0:T(2,128)(2,1)S(1)} async-done(((bf16[64,2,1024]{2,1,0:T(2,128)(2,1)}), bf16[64,2,1024]{2,1,0:T(2,128)(2,1)S(1)}, u32[]{:S(2)}, u32[]{:S(2)}) %all-to-all-start.5) | async-done | bytes 262176 | tf_op jit(solution)/shard_map/all_to_all | solution.py:18
  190.1 0.3 reshape.288
  190.5 0.6 fusion.21
  (48 shorter events, 0.9 us)
Async XLA Ops:
  0.6 154.3 %copy-start = (bf16[4096,128]{1,0:T(8,128)(2,1)S(1)}, bf16[4096,128]{1,0:T(8,128)(2,1)}, u32[]{:S(2)}) copy-start(bf16[4096,128]{1,0:T(8,128)(2,1)} %param.30) | copy-start | bytes 3145732
  58.9 0.7 copy-start.6
  59.2 1.0 copy-start.3
  59.2 1.2 copy-start.4
  59.4 1.3 copy-start.5
  59.8 0.9 copy-start.2
  62.5 8.7 %copy-start.11 = (bf16[4096,16]{0,1:T(8,128)(2,1)S(1)}, bf16[4096,16]{0,1:T(8,128)(2,1)}, u32[]{:S(2)}) copy-start(bf16[4096,16]{0,1:T(8,128)(2,1)} %param.21) | copy-start | bytes 393220
  62.5 8.7 %copy-start.13 = (f32[16]{0:T(128)S(1)}, f32[16]{0:T(128)}, u32[]{:S(2)}) copy-start(f32[16]{0:T(128)} %param.23) | copy-start | bytes 196
  62.5 9.7 %copy-start.12 = (bf16[4096,16]{0,1:T(8,128)(2,1)S(1)}, bf16[4096,16]{0,1:T(8,128)(2,1)}, u32[]{:S(2)}) copy-start(bf16[4096,16]{0,1:T(8,128)(2,1)} %param.22) | copy-start | bytes 393220
  62.5 9.7 %copy-start.14 = (f32[1,8]{1,0:T(1,128)S(1)}, f32[1,8]{1,0:T(1,128)}, u32[]{:S(2)}) copy-start(f32[1,8]{1,0:T(1,128)} %param.27) | copy-start | bytes 100
  62.5 9.6 %copy-start.15 = (f32[16]{0:T(128)S(1)}, f32[16]{0:T(128)}, u32[]{:S(2)}) copy-start(f32[16]{0:T(128)} %param.24) | copy-start | bytes 196
  63.7 26.8 %all-to-all-start = ((bf16[64,2,2048]{2,1,0:T(2,128)(2,1)}), bf16[64,2,2048]{2,1,0:T(2,128)(2,1)S(1)}, u32[]{:S(2)}, u32[]{:S(2)}) async-start(bf16[64,2,2048]{2,1,0:T(2,128)(2,1)} %reshape.279), calls=%async_computation | async-start | bytes 1048576 | tf_op jit(solution)/shard_map/all_to_all | solution.py:18
  73.2 23.3 %copy-start.9 = (f32[1,8]{1,0:T(1,128)}, f32[1,8]{1,0:T(1,128)S(1)}, u32[]{:S(2)}) copy-start(f32[1,8]{1,0:T(1,128)S(1)} %get-tuple-element.7) | copy-start | bytes 100
  73.2 21.5 %copy-start.1 = (f32[1,8,256,128]{3,2,1,0:T(8,128)S(1)}, f32[1,8,256,128]{3,2,1,0:T(8,128)}, u32[]{:S(2)}) copy-start(f32[1,8,256,128]{3,2,1,0:T(8,128)} %param.25) | copy-start | bytes 3145732
  92.3 3.4 %copy-start.8 = (f32[1,8,128]{2,1,0:T(8,128)S(1)}, f32[1,8,128]{2,1,0:T(8,128)}, u32[]{:S(2)}) copy-start(f32[1,8,128]{2,1,0:T(8,128)} %param.26) | copy-start | bytes 12292
  100.0 20.4 %all-to-all-start.1 = ((bf16[64,2,1024]{2,1,0:T(2,128)(2,1)}), bf16[64,2,1024]{2,1,0:T(2,128)(2,1)S(1)}, u32[]{:S(2)}, u32[]{:S(2)}) async-start(bf16[64,2,1024]{2,1,0:T(2,128)(2,1)} %reshape.281), calls=%async_computation.1 | async-start | bytes 524288 | tf_op jit(solution)/shard_map/all_to_all | solution.py:24
  106.0 14.6 %copy-start.10 = (bf16[2048,64]{0,1:T(8,128)(2,1)S(1)}, bf16[2048,64]{0,1:T(8,128)(2,1)}, u32[]{:S(2)}) copy-start(bf16[2048,64]{0,1:T(8,128)(2,1)} %param.28) | copy-start | bytes 786436
  127.6 24.5 %all-to-all-start.3 = ((bf16[64,2,2048]{2,1,0:T(2,128)(2,1)}), bf16[64,2,2048]{2,1,0:T(2,128)(2,1)}, u32[]{:S(2)}, u32[]{:S(2)}) async-start(bf16[64,2,2048]{2,1,0:T(2,128)(2,1)} %reshape.285), calls=%async_computation.3 | async-start | bytes 1048576 | tf_op jit(solution)/shard_map/all_to_all | solution.py:24
  135.8 19.1 %copy-start.7 = (f32[4096]{0:T(1024)S(1)}, f32[4096]{0:T(1024)}, u32[]{:S(2)}) copy-start(f32[4096]{0:T(1024)} %param.29) | copy-start | bytes 49156
  168.6 21.4 %all-to-all-start.5 = ((bf16[64,2,1024]{2,1,0:T(2,128)(2,1)}), bf16[64,2,1024]{2,1,0:T(2,128)(2,1)S(1)}, u32[]{:S(2)}, u32[]{:S(2)}) async-start(bf16[64,2,1024]{2,1,0:T(2,128)(2,1)} %reshape.287), calls=%async_computation.5 | async-start | bytes 524288 | tf_op jit(solution)/shard_map/all_to_all | solution.py:18
where the time goes:
time: 192 us; the launch traced here: 191 us
  blocking collectives  66.8 us (35%)
  waiting for transfers between devices  60.8 us (32%)
  starting transfers between devices  25.1 us (13%)
  local copies, waits for them, and re-layouts  17.3 us (9%)
  other arithmetic  12.6 us (7%)
  matrix products  7.47 us (4%)
    all_gather x1, blocking collectives, on_device(): whole_rows = lax.all_gather(tokens, ('kv', 'tp'), axis=1, tiled=True)  58.2 us
    all_to_all x2, waiting for transfers between devices, summed_on_arrival(): lax.all_to_all(cut_along(shard, dim, length), axis, 0, 0, tiled=True)  31.2 us
    all_to_all x2, waiting for transfers between devices, from_everyone(): lax.all_to_all(jnp.broadcast_to(shard[None], (length, *shard.shape)), axi...  29.6 us
    all_to_all x2, starting transfers between devices, summed_on_arrival(): lax.all_to_all(cut_along(shard, dim, length), axis, 0, 0, tiled=True)  13.6 us
    unnamed x45, local copies, waits for them, and re-layouts  12.9 us
    all_to_all x2, starting transfers between devices, from_everyone(): lax.all_to_all(jnp.broadcast_to(shard[None], (length, *shard.shape)), axi...  11.5 us
    all_to_all x1, blocking collectives, summed_on_arrival(): lax.all_to_all(cut_along(shard, dim, length), axis, 0, 0, tiled=True)  4.89 us
  transfers between devices with their start and end apart: 4, of which 4 were waited for; matrix products, arithmetic and copies ran while one was open for 4% of the time, Pallas kernels for 0%

commit v1 on v0

--- a/solution.py
+++ b/solution.py
@@ -71,7 +71,8 @@
     tp_index = lax.axis_index("tp")
     own_rows = memory.shape[0]
     head_count = memory.shape[1]
-    whole_rows = lax.all_gather(tokens, ("kv", "tp"), axis=1, tiled=True)
+    sent = jnp.stack([tokens] * lax.axis_size(("kv", "tp")))
+    whole_rows = jnp.concatenate(lax.all_to_all(sent, ("kv", "tp"), 0, 0), axis=1)
     wide_rows = whole_rows.astype(jnp.float32)
     normed = rms_normed(whole_rows, mix_gain)
     row_span = w_query.shape[0]

time: 192 us -> 173 us (0.901)
  the two profiles are of different devices: /device:TPU:4 before, /device:TPU:2 now
where the time goes in v1:
time: 173 us; the launch traced here: 172 us
  waiting for transfers between devices  83.6 us (48%)
  starting transfers between devices  41.8 us (24%)
  local copies, waits for them, and re-layouts  20.9 us (12%)
  other arithmetic  11.3 us (7%)
  blocking collectives  8.87 us (5%)
  matrix products  4.52 us (3%)
    all_to_all x2, waiting for transfers between devices, summed_on_arrival(): lax.all_to_all(cut_along(shard, dim, length), axis, 0, 0, tiled=True)  32.1 us
    all_to_all x2, waiting for transfers between devices, from_everyone(): lax.all_to_all(jnp.broadcast_to(shard[None], (length, *shard.shape)), axi...  32 us
    all_to_all x1, waiting for transfers between devices, on_device(): lax.all_to_all(sent, ('kv', 'tp'), 0, 0)  19.4 us
    all_to_all x1, starting transfers between devices, on_device(): lax.all_to_all(sent, ('kv', 'tp'), 0, 0)  17.9 us
    unnamed x51, local copies, waits for them, and re-layouts  16.3 us
    all_to_all x2, starting transfers between devices, from_everyone(): lax.all_to_all(jnp.broadcast_to(shard[None], (length, *shard.shape)), axi...  12 us
    all_to_all x2, starting transfers between devices, summed_on_arrival(): lax.all_to_all(cut_along(shard, dim, length), axis, 0, 0, tiled=True)  11.8 us
    all_to_all x1, blocking collectives, summed_on_arrival(): lax.all_to_all(cut_along(shard, dim, length), axis, 0, 0, tiled=True)  5.02 us
  transfers between devices with their start and end apart: 5, of which 5 were waited for; matrix products, arithmetic and copies ran while one was open for 2% of the time, Pallas kernels for 0%

profile of v1, /device:TPU:2, one launch (start us, length us, event | category | flops | bytes accessed | tf_op | source)
XLA Modules:
  0.0 172.0 jit_solution(4366543810143552614)
XLA Ops:
  0.6 0.9 broadcast_bitcast_fusion.1
  1.6 1.4 reshape.287
  3.0 17.9 %all-to-all-start = ((bf16[128,2,1024]{2,1,0:T(2,128)(2,1)}), bf16[128,2,1024]{2,1,0:T(2,128)(2,1)S(1)}, u32[]{:S(2)}, u32[]{:S(2)}) async-start(bf16[128,2,1024]{2,1,0:T(2,128)(2,1)} %reshape.287), calls=%async_computation | async-start | bytes 1048576 | tf_op jit(solution)/shard_map/all_to_all | solution.py:75
  20.9 19.4 %all-to-all-done = bf16[128,2,1024]{2,1,0:T(2,128)(2,1)S(1)} async-done(((bf16[128,2,1024]{2,1,0:T(2,128)(2,1)}), bf16[128,2,1024]{2,1,0:T(2,128)(2,1)S(1)}, u32[]{:S(2)}, u32[]{:S(2)}) %all-to-all-start) | async-done | bytes 524320 | tf_op jit(solution)/shard_map/all_to_all | solution.py:75
  40.3 0.6 reshape.288
  40.9 0.6 multiply_reduce_fusion.1
  41.5 1.7 multiply_convert_fusion.1
  43.2 0.3 fusion
  43.5 0.2 fusion.1
  43.7 0.2 fusion.2
  44.0 0.5 broadcast.129
  44.5 1.0 reduce.13
  45.6 1.2 reshape.289
  46.7 5.6 %all-to-all-start.1 = ((bf16[64,2,2048]{2,1,0:T(2,128)(2,1)}), bf16[64,2,2048]{2,1,0:T(2,128)(2,1)}, u32[]{:S(2)}, u32[]{:S(2)}) async-start(bf16[64,2,2048]{2,1,0:T(2,128)(2,1)} %reshape.289), calls=%async_computation.1 | async-start | bytes 1048576 | tf_op jit(solution)/shard_map/all_to_all | solution.py:18
  52.3 0.7 dynamic-slice_reduce_fusion
  53.3 0.2 bitcast_add_fusion.1
  53.5 18.2 %all-to-all-done.1 = bf16[64,2,2048]{2,1,0:T(2,128)(2,1)} async-done(((bf16[64,2,2048]{2,1,0:T(2,128)(2,1)}), bf16[64,2,2048]{2,1,0:T(2,128)(2,1)}, u32[]{:S(2)}, u32[]{:S(2)}) %all-to-all-start.1) | async-done | bytes 524320 | tf_op jit(solution)/shard_map/all_to_all | solution.py:18
  71.7 3.6 %reshape.290 = bf16[64,1,4096]{2,1,0:T(2,128)(2,1)S(1)} reshape(bf16[64,2,2048]{2,1,0:T(2,128)(2,1)} %all-to-all-done.1) | data formatting | bytes 1048576
  75.4 1.1 convert_reduce_fusion.1
  76.6 1.0 fusion.9
  77.5 0.8 multiply_reduce_fusion.3
  78.5 0.3 broadcast_in_dim.9
  78.8 2.2 %reduce.14 = bf16[64,2048]{1,0:T(8,128)(2,1)S(1)} reduce(bf16[64,1,2048]{2,1,0:T(2,128)(2,1)S(1)} %broadcast_in_dim.9, bf16[]{:T(256)} %broadcast.129), dimensions={1}, to_apply=%broadcast_in_dim.9.reduce_sub_computation | reduce | bytes 524290 | tf_op jit(solution)/shard_map/broadcast_in_dim | solution.py:25
  80.9 0.9 reshape.291
  81.8 6.5 %all-to-all-start.2 = ((bf16[64,2,1024]{2,1,0:T(2,128)(2,1)}), bf16[64,2,1024]{2,1,0:T(2,128)(2,1)S(1)}, u32[]{:S(2)}, u32[]{:S(2)}) async-start(bf16[64,2,1024]{2,1,0:T(2,128)(2,1)} %reshape.291), calls=%async_computation.2 | async-start | bytes 524288 | tf_op jit(solution)/shard_map/all_to_all | solution.py:24
  88.3 0.8 constant_dynamic-slice_fusion
  89.2 13.9 %all-to-all-done.2 = bf16[64,2,1024]{2,1,0:T(2,128)(2,1)S(1)} async-done(((bf16[64,2,1024]{2,1,0:T(2,128)(2,1)}), bf16[64,2,1024]{2,1,0:T(2,128)(2,1)S(1)}, u32[]{:S(2)}, u32[]{:S(2)}) %all-to-all-start.2) | async-done | bytes 262176 | tf_op jit(solution)/shard_map/all_to_all | solution.py:24
  103.0 0.2 reshape.292
  103.3 0.3 convolution_convert_fusion.4
  103.7 3.9 %all_to_all.35 = bf16[2,2,2048]{2,1,0:T(2,128)(2,1)S(1)} all-to-all(bf16[2,2,2048]{2,1,0:T(2,128)(2,1)S(1)} %reshape.293), channel_id=1, replica_groups=mesh['dp'=4,'kv'=64,'tp'=2] {'tp'}, dimensions={0} | all-to-all | bytes 32768 | tf_op jit(solution)/shard_map/all_to_all | solution.py:24
  107.8 0.3 broadcast_bitcast_fusion
  108.0 1.5 reshape.295
  109.6 5.5 %all-to-all-start.4 = ((bf16[64,2,2048]{2,1,0:T(2,128)(2,1)}), bf16[64,2,2048]{2,1,0:T(2,128)(2,1)}, u32[]{:S(2)}, u32[]{:S(2)}) async-start(bf16[64,2,2048]{2,1,0:T(2,128)(2,1)} %reshape.295), calls=%async_computation.4 | async-start | bytes 1048576 | tf_op jit(solution)/shard_map/all_to_all | solution.py:24
  115.1 0.7 copy.40
  115.9 18.2 %all-to-all-done.4 = bf16[64,2,2048]{2,1,0:T(2,128)(2,1)} async-done(((bf16[64,2,2048]{2,1,0:T(2,128)(2,1)}), bf16[64,2,2048]{2,1,0:T(2,128)(2,1)}, u32[]{:S(2)}, u32[]{:S(2)}) %all-to-all-start.4) | async-done | bytes 524320 | tf_op jit(solution)/shard_map/all_to_all | solution.py:24
  134.0 2.3 %reshape.296 = bf16[64,64,64]{2,1,0:T(8,128)(2,1)S(1)} reshape(bf16[64,2,2048]{2,1,0:T(2,128)(2,1)} %all-to-all-done.4) | data formatting | bytes 1048576
  136.3 0.6 multiply_reduce_fusion
  136.9 2.3 %convolution_convert_fusion = bf16[64,4096]{1,0:T(8,128)(2,1)} fusion(bf16[128,4096]{0,1:T(8,128)(2,1)S(1)} %bitcast.120, bf16[4096,128]{1,0:T(8,128)(2,1)S(1)} %copy-done, bf16[64,4096]{0,1:T(8,128)(2,1)S(1)} %bitcast.117, f32[4096]{0:T(1024)S(1)} %copy-done.8, f32[64]{0:T(128)S(1)} %add_rsqrt_fusion), kind=kOutput, calls=%fused_computation | convolution fusion | flops 135553024 | bytes 3162368 | tf_op jit(solution)/shard_map/dot_general | solution.py:139
  139.2 1.1 copy.60
  140.3 5.0 %all_to_all.36 = bf16[2,2048,64]{1,2,0:T(8,128)(2,1)} all-to-all(bf16[2,2048,64]{1,2,0:T(8,128)(2,1)S(1)} %bitcast.123), channel_id=1, replica_groups=mesh['dp'=4,'kv'=64,'tp'=2] {'tp'}, dimensions={0} | all-to-all | bytes 1048576 | tf_op jit(solution)/shard_map/all_to_all | solution.py:18
  145.3 1.1 reduce_sum.90
  146.5 1.0 copy.44
  147.5 2.1 %reshape.297 = bf16[64,2,1024]{2,1,0:T(2,128)(2,1)} reshape(bf16[64,32,64]{2,1,0:T(8,128)(2,1)} %bitcast.122) | data formatting | bytes 524288
  149.5 6.2 %all-to-all-start.6 = ((bf16[64,2,1024]{2,1,0:T(2,128)(2,1)}), bf16[64,2,1024]{2,1,0:T(2,128)(2,1)S(1)}, u32[]{:S(2)}, u32[]{:S(2)}) async-start(bf16[64,2,1024]{2,1,0:T(2,128)(2,1)} %reshape.297), calls=%async_computation.6 | async-start | bytes 524288 | tf_op jit(solution)/shard_map/all_to_all | solution.py:18
  155.8 1.3 multiply_add_fusion
  157.1 13.9 %all-to-all-done.6 = bf16[64,2,1024]{2,1,0:T(2,128)(2,1)S(1)} async-done(((bf16[64,2,1024]{2,1,0:T(2,128)(2,1)}), bf16[64,2,1024]{2,1,0:T(2,128)(2,1)S(1)}, u32[]{:S(2)}, u32[]{:S(2)}) %all-to-all-start.6) | async-done | bytes 262176 | tf_op jit(solution)/shard_map/all_to_all | solution.py:18
  171.0 0.3 reshape.298
  171.4 0.6 fusion.19
  (56 shorter events, 1.1 us)
Async XLA Ops:
  0.6 136.3 %copy-start = (bf16[4096,128]{1,0:T(8,128)(2,1)S(1)}, bf16[4096,128]{1,0:T(8,128)(2,1)}, u32[]{:S(2)}) copy-start(bf16[4096,128]{1,0:T(8,128)(2,1)} %param.30) | copy-start | bytes 3145732
  3.0 38.5 %copy-start.7 = (f32[4096]{0:T(1024)S(1)}, f32[4096]{0:T(1024)}, u32[]{:S(2)}) copy-start(f32[4096]{0:T(1024)} %param.17) | copy-start | bytes 49156
  3.0 37.4 %all-to-all-start = ((bf16[128,2,1024]{2,1,0:T(2,128)(2,1)}), bf16[128,2,1024]{2,1,0:T(2,128)(2,1)S(1)}, u32[]{:S(2)}, u32[]{:S(2)}) async-start(bf16[128,2,1024]{2,1,0:T(2,128)(2,1)} %reshape.287), calls=%async_computation | async-start | bytes 1048576 | tf_op jit(solution)/shard_map/all_to_all | solution.py:75
  41.5 1.7 copy-start.4
  41.5 2.0 %copy-start.5 = (bf16[64,1024]{1,0:T(8,128)(2,1)S(1)}, bf16[64,1024]{1,0:T(8,128)(2,1)}, u32[]{:S(2)}) copy-start(bf16[64,1024]{1,0:T(8,128)(2,1)} %param.18) | copy-start | bytes 393220
  41.5 2.2 %copy-start.6 = (bf16[64,1024]{1,0:T(8,128)(2,1)S(1)}, bf16[64,1024]{1,0:T(8,128)(2,1)}, u32[]{:S(2)}) copy-start(bf16[64,1024]{1,0:T(8,128)(2,1)} %param.19) | copy-start | bytes 393220
  44.5 8.6 %copy-start.12 = (bf16[4096,16]{0,1:T(8,128)(2,1)S(1)}, bf16[4096,16]{0,1:T(8,128)(2,1)}, u32[]{:S(2)}) copy-start(bf16[4096,16]{0,1:T(8,128)(2,1)} %param.21) | copy-start | bytes 393220
  44.5 8.6 %copy-start.14 = (f32[16]{0:T(128)S(1)}, f32[16]{0:T(128)}, u32[]{:S(2)}) copy-start(f32[16]{0:T(128)} %param.23) | copy-start | bytes 196
  44.5 8.8 %copy-start.13 = (bf16[4096,16]{0,1:T(8,128)(2,1)S(1)}, bf16[4096,16]{0,1:T(8,128)(2,1)}, u32[]{:S(2)}) copy-start(bf16[4096,16]{0,1:T(8,128)(2,1)} %param.22) | copy-start | bytes 393220
  44.5 8.8 %copy-start.15 = (f32[1,8]{1,0:T(1,128)S(1)}, f32[1,8]{1,0:T(1,128)}, u32[]{:S(2)}) copy-start(f32[1,8]{1,0:T(1,128)} %param.27) | copy-start | bytes 100
  44.5 8.8 %copy-start.16 = (f32[16]{0:T(128)S(1)}, f32[16]{0:T(128)}, u32[]{:S(2)}) copy-start(f32[16]{0:T(128)} %param.24) | copy-start | bytes 196
  46.7 25.0 %all-to-all-start.1 = ((bf16[64,2,2048]{2,1,0:T(2,128)(2,1)}), bf16[64,2,2048]{2,1,0:T(2,128)(2,1)}, u32[]{:S(2)}, u32[]{:S(2)}) async-start(bf16[64,2,2048]{2,1,0:T(2,128)(2,1)} %reshape.289), calls=%async_computation.1 | async-start | bytes 1048576 | tf_op jit(solution)/shard_map/all_to_all | solution.py:18
  52.3 24.2 %copy-start.1 = (f32[1,8,256,128]{3,2,1,0:T(8,128)S(1)}, f32[1,8,256,128]{3,2,1,0:T(8,128)}, u32[]{:S(2)}) copy-start(f32[1,8,256,128]{3,2,1,0:T(8,128)} %param.25) | copy-start | bytes 3145732
  53.1 24.5 %copy-start.9 = (f32[1,8,128]{2,1,0:T(8,128)S(1)}, f32[1,8,128]{2,1,0:T(8,128)}, u32[]{:S(2)}) copy-start(f32[1,8,128]{2,1,0:T(8,128)} %param.26) | copy-start | bytes 12292
  53.5 25.3 %copy-start.10 = (f32[1,8]{1,0:T(1,128)}, f32[1,8]{1,0:T(1,128)S(1)}, u32[]{:S(2)}) copy-start(f32[1,8]{1,0:T(1,128)S(1)} %get-tuple-element.7) | copy-start | bytes 100
  76.6 26.7 %copy-start.11 = (bf16[2048,64]{0,1:T(8,128)(2,1)S(1)}, bf16[2048,64]{0,1:T(8,128)(2,1)}, u32[]{:S(2)}) copy-start(bf16[2048,64]{0,1:T(8,128)(2,1)} %param.28) | copy-start | bytes 786436
  81.8 21.2 %all-to-all-start.2 = ((bf16[64,2,1024]{2,1,0:T(2,128)(2,1)}), bf16[64,2,1024]{2,1,0:T(2,128)(2,1)S(1)}, u32[]{:S(2)}, u32[]{:S(2)}) async-start(bf16[64,2,1024]{2,1,0:T(2,128)(2,1)} %reshape.291), calls=%async_computation.2 | async-start | bytes 524288 | tf_op jit(solution)/shard_map/all_to_all | solution.py:24
  103.6 11.5 %copy-start.3 = (bf16[128,4096]{1,0:T(8,128)(2,1)S(1)}, bf16[128,4096]{1,0:T(8,128)(2,1)}, u32[]{:S(2)}) copy-start(bf16[128,4096]{1,0:T(8,128)(2,1)} %param.31) | copy-start | bytes 3145732
  109.6 24.5 %all-to-all-start.4 = ((bf16[64,2,2048]{2,1,0:T(2,128)(2,1)}), bf16[64,2,2048]{2,1,0:T(2,128)(2,1)}, u32[]{:S(2)}, u32[]{:S(2)}) async-start(bf16[64,2,2048]{2,1,0:T(2,128)(2,1)} %reshape.295), calls=%async_computation.4 | async-start | bytes 1048576 | tf_op jit(solution)/shard_map/all_to_all | solution.py:24
  115.8 21.1 %copy-start.8 = (f32[4096]{0:T(1024)S(1)}, f32[4096]{0:T(1024)}, u32[]{:S(2)}) copy-start(f32[4096]{0:T(1024)} %param.29) | copy-start | bytes 49156
  140.3 15.5 %copy-start.2 = (f32[1,8,256,128]{3,2,1,0:T(8,128)S(1)}, f32[1,8,256,128]{3,2,1,0:T(8,128)}, u32[]{:S(2)}) copy-start(f32[1,8,256,128]{3,2,1,0:T(8,128)} %param.25) | copy-start | bytes 3145732
  149.5 21.4 %all-to-all-start.6 = ((bf16[64,2,1024]{2,1,0:T(2,128)(2,1)}), bf16[64,2,1024]{2,1,0:T(2,128)(2,1)S(1)}, u32[]{:S(2)}, u32[]{:S(2)}) async-start(bf16[64,2,1024]{2,1,0:T(2,128)(2,1)} %reshape.297), calls=%async_computation.6 | async-start | bytes 524288 | tf_op jit(solution)/shard_map/all_to_all | solution.py:18
